TPU v7x, 32 devices: a whole 2x2x4 slice. The times are simulated.
32 devices in a mesh: fs: 8 (over z, y), tp: 4 (over x, core).
Axes of the slice: x: 2, y: 2, z: 4, core: 2. Of those that a mesh axis runs over, the one named last changes fastest.
Arguments:
- query_latent_rows: bfloat16 [12288, 1024], P('fs'), may hold values from -6 to 6
- grad_q: bfloat16 [12288, 3072], P('fs', 'tp'), may hold values from -6 to 6
- head_out: bfloat16 [12288, 2048], P('fs', 'tp'), may hold values from -6 to 6
- grad_out: bfloat16 [12288, 4096], P('fs'), may hold values from -6 to 6
- proj_q: bfloat16 [1024, 256], P('fs'), may hold values from -0.5 to 0.5
- proj_o: bfloat16 [4096, 256], P('fs'), may hold values from -0.5 to 0.5
- query_up_weight: float32 [1024, 3072], P('fs', 'tp'), may hold values from -0.1875 to 0.1875
- weight_o: float32 [4096, 2048], P('fs', 'tp'), may hold values from -0.125 to 0.125
- first_q: float32 [256, 3072], P('fs', 'tp'), may hold values from -6 to 6
- second_q: float32 [256, 3072], P('fs', 'tp'), may hold values from 0.25 to 4
- first_o: float32 [256, 2048], P('fs', 'tp'), may hold values from -6 to 6
- second_o: float32 [256, 2048], P('fs', 'tp'), may hold values from 0.25 to 4
Outputs:
- new_weight_q: float32 [1024, 3072], P('fs', 'tp')
- new_weight_o: float32 [4096, 2048], P('fs', 'tp')
- new_first_q: float32 [256, 3072], P('fs', 'tp')
- new_second_q: float32 [256, 3072], P('fs', 'tp')
- new_first_o: float32 [256, 2048], P('fs', 'tp')
- new_second_o: float32 [256, 2048], P('fs', 'tp')
- step_q: float32 [1024, 3072], P('fs', 'tp')
- step_o: float32 [4096, 2048], P('fs', 'tp')
- copy_q: bfloat16 [1024, 3072], P(None, 'tp')
- copy_o: bfloat16 [4096, 2048], P(None, 'tp')
All inputs are finite; a program needn't handle non-finite values.
Results may differ from a plain program's by a relative error of at most 0.008.
Values may be sent and summed in bfloat16 or wider, within the bound.
A program may use at most 128 MiB of HBM per device.

v0:
```python
import math

import jax
import jax.numpy as jnp
from jax import lax
from jax.sharding import PartitionSpec as P

beta_first = 0.8
beta_second = 0.9
epsilon = 1e-08
decay_rate = 2.0
step_rate = 0.05
contract = (((0,), (0,)), ((), ()))


def tokens_product(left, right):
    return lax.dot_general(left, right, contract, preferred_element_type=jnp.float32)


def exact_product(basis_column_count, gradient):
    return lax.dot_general(
        basis_column_count.astype(jnp.float32),
        gradient,
        contract,
        precision=lax.Precision.HIGHEST,
        preferred_element_type=jnp.float32,
    )


def moments(first, second, reduced, clip_scale):
    scaled = clip_scale * reduced
    first_new = beta_first * first + (1.0 - beta_first) * scaled
    second_new = beta_second * second + (1.0 - beta_second) * scaled * scaled
    return (first_new, second_new, first_new / (jnp.sqrt(second_new) + epsilon))


def per_device(
    query_latent_rows,
    grad_q,
    head_out,
    grad_out,
    proj_q,
    proj_o,
    query_up_weight,
    weight_o,
    first_q,
    second_q,
    first_o,
    second_o,
):
    rank_rows = first_q.shape[0]
    whole_q, whole_o = (
        lax.all_gather(proj_q, "fs", axis=0, tiled=True),
        lax.all_gather(proj_o, "fs", axis=0, tiled=True),
    )
    partial_q = tokens_product(query_latent_rows, grad_q)
    partial_o = tokens_product(grad_out, head_out)
    low_q = lax.psum_scatter(
        exact_product(whole_q, partial_q).astype(jnp.bfloat16),
        "fs",
        scatter_dimension=0,
        tiled=True,
    ).astype(jnp.float32)
    low_o = lax.psum_scatter(
        exact_product(whole_o, partial_o).astype(jnp.bfloat16),
        "fs",
        scatter_dimension=0,
        tiled=True,
    ).astype(jnp.float32)
    sum_squares = lax.psum(jnp.sum(low_q * low_q) + jnp.sum(low_o * low_o), ("fs", "tp"))
    entries = (
        rank_rows
        * lax.axis_size("fs")
        * (first_q.shape[1] + first_o.shape[1])
        * lax.axis_size("tp")
    )
    clip_scale = jnp.minimum(1.0, math.sqrt(entries) / jnp.sqrt(sum_squares))
    first_nq, second_nq, direct_q = moments(first_q, second_q, low_q, clip_scale)
    first_no, second_no, direct_o = moments(first_o, second_o, low_o, clip_scale)
    basis_q = proj_q.astype(jnp.float32)
    basis_o = proj_o.astype(jnp.float32)
    more_q = jnp.dot(
        basis_q,
        lax.all_gather(direct_q, "fs", axis=0, tiled=True),
        precision=lax.Precision.HIGHEST,
        preferred_element_type=jnp.float32,
    )
    more_o = jnp.dot(
        basis_o,
        lax.all_gather(direct_o, "fs", axis=0, tiled=True),
        precision=lax.Precision.HIGHEST,
        preferred_element_type=jnp.float32,
    )
    step_q = more_q + decay_rate * query_up_weight
    step_o = more_o + decay_rate * weight_o
    new_weight_q = query_up_weight - step_rate * step_q
    new_weight_o = weight_o - step_rate * step_o
    copy_q, copy_o = (
        lax.all_gather(new_weight_q.astype(jnp.bfloat16), "fs", axis=0, tiled=True),
        lax.all_gather(new_weight_o.astype(jnp.bfloat16), "fs", axis=0, tiled=True),
    )
    return (
        new_weight_q,
        new_weight_o,
        first_nq,
        second_nq,
        first_no,
        second_no,
        step_q,
        step_o,
        copy_q,
        copy_o,
    )


def solution(mesh):
    return jax.shard_map(
        per_device,
        mesh=mesh,
        in_specs=(
            P("fs", None),
            P("fs", "tp"),
            P("fs", "tp"),
            P("fs", None),
            P("fs", None),
            P("fs", None),
            P("fs", "tp"),
            P("fs", "tp"),
            P("fs", "tp"),
            P("fs", "tp"),
            P("fs", "tp"),
            P("fs", "tp"),
        ),
        out_specs=(
            P("fs", "tp"),
            P("fs", "tp"),
            P("fs", "tp"),
            P("fs", "tp"),
            P("fs", "tp"),
            P("fs", "tp"),
            P("fs", "tp"),
            P("fs", "tp"),
            P(None, "tp"),
            P(None, "tp"),
        ),
        check_vma=False,
    )
```

profile of v0, /device:TPU:0, one launch (start us, length us, event | category | flops | bytes accessed | tf_op | source)
XLA Modules:
  0.0 410.3 jit_solution(11998339076811375479)
XLA Ops:
  8.0 34.2 %all_gather.18 = bf16[1024,256]{1,0:T(8,128)(2,1)S(1)} all-gather(bf16[128,256]{1,0:T(8,128)(2,1)} %param.16), channel_id=1, replica_groups=mesh['fs'=8,'tp'=4] {'fs'}, dimensions={0}, use_global_device_ids=true | all-gather | bytes 589824 | tf_op jit(solution)/shard_map/all_gather | solution.py:53
  42.2 4.4 %fusion.18 = f32[1024,768]{1,0:T(8,128)S(1)} fusion(bf16[1536,1024]{1,0:T(8,128)(2,1)S(1)} %copy-done, bf16[1536,768]{1,0:T(8,128)(2,1)} %param.13), kind=kOutput, calls=%fused_computation.28 | convolution fusion | flops 2415919104 | bytes 8650752 | tf_op jit(solution)/shard_map/dot_general | solution.py:17
  46.6 2.7 fusion.1
  50.4 12.2 %fusion.19 = f32[4096,512]{1,0:T(8,128)} fusion(bf16[1536,4096]{1,0:T(8,128)(2,1)} %param.15, bf16[1536,512]{1,0:T(8,128)(2,1)} %param.14), kind=kOutput, calls=%fused_computation.29 | convolution fusion | flops 6442450944 | bytes 22544384 | tf_op jit(solution)/shard_map/dot_general | solution.py:17
  63.3 10.6 %fusion.3 = bf16[256,512]{0,1:T(8,128)(2,1)S(1)} fusion(f32[4096,512]{1,0:T(8,128)} %fusion.19, bf16[4096,256]{1,0:T(8,128)(2,1)} %all-gather.4.cloned.1.call-done), kind=kOutput, calls=%fused_computation.7 | convolution fusion | flops 6442582016 | bytes 10747904 | tf_op jit(solution)/shard_map/dot_general | solution.py:21
  74.8 53.3 %reduce-scatter.7.cloned.1.call-done = bf16[32,768]{1,0:T(8,128)(2,1)} async-done(((bf16[256,768]{1,0:T(8,128)(2,1)}), bf16[32,768]{1,0:T(8,128)(2,1)}) %reduce-scatter.7.cloned.1.call-update) | async-done | bytes 49168 | tf_op jit(solution)/shard_map/reduce_scatter | solution.py:58
  128.1 1.4 fusion.6
  129.5 63.7 %reduce-scatter.9.cloned.1.call-done = bf16[32,512]{1,0:T(8,128)(2,1)} async-done(((bf16[256,512]{1,0:T(8,128)(2,1)}), bf16[32,512]{1,0:T(8,128)(2,1)}) %reduce-scatter.9.cloned.1.call-update) | async-done | bytes 32784 | tf_op jit(solution)/shard_map/reduce_scatter | solution.py:64
  193.2 1.4 fusion.10
  195.8 1.9 copy.63
  197.8 40.1 %psum.7 = f32[]{:T(128)} all-reduce(f32[]{:T(128)S(6)} %add.39), channel_id=1, replica_groups=mesh['fs'=8,'tp'=4] {'fs','tp'}, use_global_device_ids=true, to_apply=%region_4.0 | all-reduce | flops 1 | bytes 8 | tf_op jit(solution)/shard_map/psum | solution.py:70
  238.5 1.7 add_divide_fusion
  240.2 32.1 %all_gather.20 = f32[256,768]{1,0:T(8,128)S(1)} all-gather(f32[32,768]{1,0:T(8,128)S(1)} %get-tuple-element.47), channel_id=1, replica_groups=mesh['fs'=8,'tp'=4] {'fs'}, dimensions={0}, use_global_device_ids=true | all-gather | bytes 884736 | tf_op jit(solution)/shard_map/all_gather | solution.py:84
  272.2 2.7 fusion.13
  275.0 2.5 copy.65
  277.5 1.6 add_divide_fusion.1
  279.1 32.8 %all_gather.21 = f32[256,512]{1,0:T(8,128)S(1)} all-gather(f32[32,512]{1,0:T(8,128)S(1)} %get-tuple-element.44), channel_id=1, replica_groups=mesh['fs'=8,'tp'=4] {'fs'}, dimensions={0}, use_global_device_ids=true | all-gather | bytes 589824 | tf_op jit(solution)/shard_map/all_gather | solution.py:90
  311.9 3.9 fusion.12
  315.8 2.5 copy.67
  318.3 2.5 copy.69
  320.9 1.9 copy.66
  323.7 2.6 copy.70
  326.3 71.1 %all-gather.8.cloned.1.call-done = bf16[4096,512]{0,1:T(8,128)(2,1)} async-done(((bf16[512,512]{0,1:T(8,128)(2,1)}), bf16[4096,512]{0,1:T(8,128)(2,1)}) %all-gather.8.cloned.1.call-update) | async-done | bytes 4194320 | tf_op jit(solution)/shard_map/all_gather | solution.py:100
  397.4 6.4 %copy.71 = bf16[4096,512]{1,0:T(8,128)(2,1)} copy(bf16[4096,512]{0,1:T(8,128)(2,1)} %all-gather.8.cloned.1.call-done) | data formatting | bytes 8388608
  (19 shorter events, 4.5 us)
Async XLA Ops:
  7.2 35.0 %copy-start = (bf16[1536,1024]{1,0:T(8,128)(2,1)S(1)}, bf16[1536,1024]{1,0:T(8,128)(2,1)}, u32[]{:S(2)}) copy-start(bf16[1536,1024]{1,0:T(8,128)(2,1)} %param.12) | copy-start | bytes 9437188
  7.2 56.1 %all-gather.4.cloned.1.call-start = ((), (), s32[]{:S(2)}) async-start(), calls=%async_computation.2 | async-start | bytes 2359296 | tf_op jit(solution)/shard_map/all_gather | solution.py:54
  7.9 120.1 %reduce-scatter.7.cloned.1.call-start = ((), (), s32[]{:S(2)}) async-start(), calls=%async_computation.5 | async-start | bytes 442368 | tf_op jit(solution)/shard_map/reduce_scatter | solution.py:58
  50.2 143.0 %reduce-scatter.9.cloned.1.call-start = ((), (), s32[]{:S(2)}) async-start(), calls=%async_computation.6 | async-start | bytes 294912 | tf_op jit(solution)/shard_map/reduce_scatter | solution.py:64
  62.6 175.9 %copy-start.1 = (f32[32,768]{1,0:T(8,128)S(1)}, f32[32,768]{1,0:T(8,128)}, u32[]{:S(2)}) copy-start(f32[32,768]{1,0:T(8,128)} %param.21) | copy-start | bytes 294916
  74.8 248.9 %all-gather.6.cloned.1.call-start = ((), (), s32[]{:S(2)}) async-start(), calls=%async_computation.3 | async-start | bytes 1769472 | tf_op jit(solution)/shard_map/all_gather | solution.py:99
  274.9 122.4 %all-gather.8.cloned.1.call-start = ((), (), s32[]{:S(2)}) async-start(), calls=%async_computation.4 | async-start | bytes 4718592 | tf_op jit(solution)/shard_map/all_gather | solution.py:100
Sparse Core Ops, SparseCore 0:
  10.1 53.0 all-gather.3
  67.1 60.9 reduce-scatter.6
  132.0 61.1 reduce-scatter.8
  275.1 46.4 all-gather.5
  324.0 73.2 all-gather.7
where the time goes:
time: 411 us; the launch traced here: 410 us
  waiting for transfers between devices  189 us (46%)
  blocking collectives  139 us (34%)
  matrix products  36.5 us (9%)
  local copies, waits for them, and re-layouts  23.1 us (6%)
  between operations  15.8 us (4%)
  other arithmetic  6.04 us (1%)
    all_gather x1, waiting for transfers between devices, per_device(): lax.all_gather(new_weight_o.astype(jnp.bfloat16), 'fs', axis=0, tiled=True)  71.1 us
    reduce_scatter x1, waiting for transfers between devices, per_device(): lax.psum_scatter(exact_product(whole_o, partial_o).astype(jnp.bfloat16),...  63.7 us
    reduce_scatter x1, waiting for transfers between devices, per_device(): lax.psum_scatter(exact_product(whole_q, partial_q).astype(jnp.bfloat16),...  53.3 us
    psum x1, blocking collectives, per_device(): lax.psum(jnp.sum(low_q * low_q) + jnp.sum(low_o * low_o), ('fs', 'tp'))  40.1 us
    all_gather x1, blocking collectives, per_device(): lax.all_gather(proj_q, 'fs', axis=0, tiled=True)  34.2 us
    all_gather x1, blocking collectives, per_device(): lax.all_gather(direct_o, 'fs', axis=0, tiled=True)  32.8 us
    all_gather x1, blocking collectives, per_device(): lax.all_gather(direct_q, 'fs', axis=0, tiled=True)  32.1 us
    unnamed x14, local copies, waits for them, and re-layouts  23.1 us
  transfers between devices with their start and end apart: 5, of which 4 were waited for; matrix products, arithmetic and copies ran while one was open for 13% of the time, Pallas kernels for 0%

commit v1 on v0

v1 whole, which is shorter than its diff:
```python
import functools
import math

import jax
import jax.numpy as jnp
from jax import lax
from jax.experimental import pallas as pl
from jax.experimental.pallas import tpu as pltpu
from jax.sharding import PartitionSpec as P

beta_first = 0.8
beta_second = 0.9
epsilon = 1e-08
decay_rate = 2.0
step_rate = 0.05
f32 = jnp.float32
bf16 = jnp.bfloat16
MESH = pl.DeviceIdType.MESH


def moments(first, second, scaled):
    first_new = beta_first * first + (1.0 - beta_first) * scaled
    second_new = beta_second * second + (1.0 - beta_second) * scaled * scaled
    return (first_new, second_new, first_new / (jnp.sqrt(second_new) + epsilon))


def kernel(
    n,
    tps,
    s,
    entries,
    tile,
    ql_hbm,
    gq_hbm,
    ho_hbm,
    go_hbm,
    pq_in,
    po_in,
    wq_in,
    wo_in,
    first_in,
    second_in,
    wq_all,
    wo_all,
    pq_all,
    po_all,
    dir_all,
    scaled_out,
    ql,
    gq,
    ho,
    go,
    tq,
    to,
    low_send,
    low_recv,
    dir_own,
    ss_fs,
    ss_tp,
    ss_own,
    load_sem,
    p1_send,
    p1_recv,
    p2_send,
    p2_recv,
    w_send,
    w_recv,
    rs_send,
    rs_recv,
    sf_send,
    sf_recv,
    st_send,
    st_recv,
    d_send,
    d_recv,
):
    f = lax.axis_index("fs")
    t = lax.axis_index("tp")
    fs_peer = [lax.rem(f + k, n) for k in range(n)]
    fs_from = [lax.rem(f + n - k, n) for k in range(n)]
    tp_peer = [lax.rem(t + k, tps) for k in range(tps)]
    tp_from = [lax.rem(t + tps - k, tps) for k in range(tps)]
    mine = lax.rem(t, s)
    group = t - mine

    loads = [
        pltpu.make_async_copy(src, dst, load_sem.at[i])
        for i, (src, dst) in enumerate(((go_hbm, go), (ho_hbm, ho), (ql_hbm, ql), (gq_hbm, gq)))
    ]
    for load in loads:
        load.start()

    barrier = pltpu.get_barrier_semaphore()
    for k in range(1, n):
        pl.semaphore_signal(barrier, inc=1, device_id=(fs_peer[k], t), device_id_type=MESH)
    for k in range(1, tps):
        pl.semaphore_signal(barrier, inc=1, device_id=(f, tp_peer[k]), device_id_type=MESH)
    pl.semaphore_wait(barrier, n + tps - 2)

    def send(src, dst, send_sem, recv_sem, device):
        copy = pltpu.make_async_remote_copy(
            src_ref=src,
            dst_ref=dst,
            send_sem=send_sem,
            recv_sem=recv_sem,
            device_id=device,
            device_id_type=MESH,
        )
        copy.start()
        return copy

    pairs = ((pq_in, pq_all), (po_in, po_all))
    first_hop = []
    for k in range(1, n):
        first_hop.append(
            [
                send(own.at[mine], whole.at[f, mine], p1_send.at[i, k], p1_recv.at[i, k], (fs_peer[k], t))
                for i, (own, whole) in enumerate(pairs)
            ]
        )

    depth = min(4, n)
    width = n // depth
    row, column = f // width, lax.rem(f, width)
    place = column * depth + row + lax.rem(column, 2) * (depth - 1 - 2 * row)

    def at_place(p):
        p = lax.rem(p + 2 * n, n)
        y = p // depth
        r = lax.rem(p, depth)
        return (r + lax.rem(y, 2) * (depth - 1 - 2 * r)) * width + y

    weights = ((wq_in, wq_all), (wo_in, wo_all))
    ring = []

    def ring_step(step):
        if step > 0:
            for copy in ring[step - 1]:
                copy.wait_recv()
        if step > n - 2:
            return
        copies = []
        for i, (own, whole) in enumerate(weights):
            half = own.shape[0] // 2
            for way, sign in enumerate((1, -1)):
                rows = pl.ds(way * half, half)
                owner = at_place(place - sign * step)
                source = own.at[rows] if step == 0 else whole.at[owner, rows]
                copies.append(
                    send(
                        source,
                        whole.at[owner, rows],
                        w_send.at[step, i, way],
                        w_recv.at[step, i, way],
                        (at_place(place + sign), t),
                    )
                )
        ring.append(copies)

    ring_step(0)
    for own, whole in weights + pairs:
        whole[f] = own[...]

    second_hop = []
    for k in range(1, n):
        for copy in first_hop[k - 1]:
            copy.wait_recv()
        for j in range(1, s):
            target = group + lax.rem(mine + j, s)
            for i, (own, whole) in enumerate(pairs):
                slot = whole.at[fs_from[k], mine]
                second_hop.append(
                    send(slot, slot, p2_send.at[i, k, j], p2_recv.at[i, k, j], (f, target))
                )
    for load in loads:
        load.wait()
    for copy in second_hop:
        copy.wait_recv()
    ring_step(1)

    tokens = go.shape[0]
    ro = po_all.shape[2] * s
    rank = pq_all.shape[3]

    @pl.loop(0, tokens // tile)
    def _(i):
        at = pl.ds(pl.multiple_of(i * tile, tile), tile)
        acc = jnp.zeros((tile, rank), f32)
        for b in range(n):
            acc += jnp.dot(
                go[at, b * ro : (b + 1) * ro],
                po_all[b].reshape(ro, rank),
                preferred_element_type=f32,
            )
        to[:, at] = acc.T.astype(bf16)
        acc = jnp.dot(ql[at, :], pq_all[...].reshape(-1, rank), preferred_element_type=f32)
        tq[:, at] = acc.T.astype(bf16)

    cq = gq.shape[1]
    co = ho.shape[1]
    rr = low_send.shape[1]
    for left, right, base in ((tq, gq, 0), (to, ho, cq)):
        for c in range(0, right.shape[1], 128):
            part = jnp.dot(left[...], right[:, c : c + 128], preferred_element_type=f32)
            low_send[:, :, base + c : base + c + 128] = part.astype(bf16).reshape(n, rr, 128)

    scatter = [
        send(low_send.at[fs_peer[k]], low_recv.at[f], rs_send.at[k], rs_recv.at[k], (fs_peer[k], t))
        for k in range(1, n)
    ]
    low_recv[f] = low_send[f]
    ring_step(2)
    for copy in scatter:
        copy.wait_recv()
    low = low_recv[0].astype(f32)
    for b in range(1, n):
        low += low_recv[b].astype(f32)
    ss_own[...] = jnp.broadcast_to(jnp.sum(low * low, keepdims=True), ss_own.shape)
    sums = [
        send(ss_own, ss_fs.at[f], sf_send.at[k], sf_recv.at[k], (fs_peer[k], t)) for k in range(1, n)
    ]
    ss_fs[f] = ss_own[...]
    for copy in sums:
        copy.wait_recv()
    ss_tp[t] = jnp.sum(ss_fs[...], axis=0)
    sums_tp = [
        send(ss_tp.at[t], ss_tp.at[t], st_send.at[k], st_recv.at[k], (f, tp_peer[k]))
        for k in range(1, tps)
    ]
    ring_step(3)
    for copy in sums_tp:
        copy.wait_recv()
    total = jnp.sum(ss_tp[...], axis=0)[0:1, 0:1]
    clip_scale = jnp.minimum(1.0, math.sqrt(entries) / jnp.sqrt(total))
    scaled = clip_scale * low
    scaled_out[...] = scaled
    _, _, direct = moments(first_in[...], second_in[...], scaled)
    dir_own[...] = direct.astype(bf16)
    spread = [
        send(dir_own, dir_all.at[f], d_send.at[k], d_recv.at[k], (fs_peer[k], t)) for k in range(1, n)
    ]
    dir_all[f] = dir_own[...]
    for step in range(4, n):
        ring_step(step)
    for copy in spread:
        copy.wait_recv()
    for group_of in (*first_hop, second_hop, *ring, scatter, sums, sums_tp, spread):
        for copy in group_of:
            copy.wait_send()


def per_device(
    n,
    tps,
    query_latent_rows,
    grad_q,
    head_out,
    grad_out,
    proj_q,
    proj_o,
    query_up_weight,
    weight_o,
    first_q,
    second_q,
    first_o,
    second_o,
):
    rq, rank = proj_q.shape
    ro = proj_o.shape[0]
    cq, co = grad_q.shape[1], head_out.shape[1]
    rr = first_q.shape[0]
    tokens = grad_out.shape[0]
    columns = cq + co
    s = math.gcd(tps, rq // 16)
    tile = math.gcd(tokens, 256)
    entries = rr * n * columns * tps
    first = jnp.concatenate([first_q, first_o], axis=1)
    second = jnp.concatenate([second_q, second_o], axis=1)
    wq = query_up_weight.astype(bf16)
    wo = weight_o.astype(bf16)
    vmem = pl.BlockSpec(memory_space=pltpu.VMEM)
    hbm = pl.BlockSpec(memory_space=pl.ANY)
    dma = pltpu.SemaphoreType.DMA
    wq_all, wo_all, pq_all, po_all, dir_all, scaled = pl.pallas_call(
        functools.partial(kernel, n, tps, s, entries, tile),
        out_shape=(
            jax.ShapeDtypeStruct((n, rq, cq), bf16),
            jax.ShapeDtypeStruct((n, ro, co), bf16),
            jax.ShapeDtypeStruct((n, s, rq // s, rank), bf16),
            jax.ShapeDtypeStruct((n, s, ro // s, rank), bf16),
            jax.ShapeDtypeStruct((n, rr, columns), bf16),
            jax.ShapeDtypeStruct((rr, columns), f32),
        ),
        in_specs=[hbm] * 4 + [vmem] * 6,
        out_specs=(vmem,) * 6,
        scratch_shapes=[
            pltpu.VMEM(query_latent_rows.shape, bf16),
            pltpu.VMEM(grad_q.shape, bf16),
            pltpu.VMEM(head_out.shape, bf16),
            pltpu.VMEM(grad_out.shape, bf16),
            pltpu.VMEM((rank, tokens), bf16),
            pltpu.VMEM((rank, tokens), bf16),
            pltpu.VMEM((n, rr, columns), bf16),
            pltpu.VMEM((n, rr, columns), bf16),
            pltpu.VMEM((rr, columns), bf16),
            pltpu.VMEM((n, 8, 128), f32),
            pltpu.VMEM((tps, 8, 128), f32),
            pltpu.VMEM((8, 128), f32),
            dma((4,)),
            dma((2, n)),
            dma((2, n)),
            dma((2, n, s)),
            dma((2, n, s)),
            dma((n - 1, 2, 2)),
            dma((n - 1, 2, 2)),
            dma((n,)),
            dma((n,)),
            dma((n,)),
            dma((n,)),
            dma((tps,)),
            dma((tps,)),
            dma((n,)),
            dma((n,)),
        ],
        compiler_params=pltpu.CompilerParams(
            collective_id=0, has_side_effects=True, vmem_limit_bytes=60 * 1024 * 1024
        ),
    )(
        query_latent_rows,
        grad_q,
        head_out,
        grad_out,
        proj_q.reshape(s, rq // s, rank),
        proj_o.reshape(s, ro // s, rank),
        wq,
        wo,
        first,
        second,
    )
    direct = dir_all.reshape(rank, columns)
    direct_q, direct_o = direct[:, :cq], direct[:, cq:]
    first_nq, second_nq, _ = moments(first_q, second_q, scaled[:, :cq])
    first_no, second_no, _ = moments(first_o, second_o, scaled[:, cq:])

    def update(basis, directions, weight):
        step = jnp.dot(basis, directions, preferred_element_type=f32) + decay_rate * weight
        return step, weight - step_rate * step

    step_q, new_weight_q = update(proj_q, direct_q, query_up_weight)
    step_o, new_weight_o = update(proj_o, direct_o, weight_o)
    _, copy_q = update(pq_all.reshape(n * rq, rank), direct_q, wq_all.reshape(n * rq, cq).astype(f32))
    _, copy_o = update(po_all.reshape(n * ro, rank), direct_o, wo_all.reshape(n * ro, co).astype(f32))
    return (
        new_weight_q,
        new_weight_o,
        first_nq,
        second_nq,
        first_no,
        second_no,
        step_q,
        step_o,
        copy_q.astype(bf16),
        copy_o.astype(bf16),
    )


def solution(mesh):
    both = P("fs", "tp")
    rows = P("fs", None)
    return jax.shard_map(
        functools.partial(per_device, mesh.shape["fs"], mesh.shape["tp"]),
        mesh=mesh,
        in_specs=(rows, both, both, rows, rows, rows) + (both,) * 6,
        out_specs=(both,) * 8 + (P(None, "tp"),) * 2,
        check_vma=False,
    )
```

time: 411 us -> 148 us (0.36)
  waiting for transfers between devices: 189 us -> 0 us
  blocking collectives: 139 us -> 0 us
  Pallas kernels: 0 us -> 124 us
  matrix products: 36.5 us -> 10.4 us
  local copies, waits for them, and re-layouts: 23.1 us -> 4.98 us
  between operations: 15.8 us -> 0.78 us
    pallas_call x0 -> x1, Pallas kernels: none -> 124 us  [per_device(): pl.pallas_call(functools.partial(kernel, n, tps, s, entries, tile), out_s...]
    reduce_scatter x2 -> x0, waiting for transfers between devices: 117 us -> none  [the longest x1 63.7 us: per_device(): lax.psum_scatter(exact_product(whole_o, partial_o).astype(jnp.bfloat16),...]
    all_gather x3 -> x0, blocking collectives: 99 us -> none  [the longest x1 34.2 us: per_device(): lax.all_gather(proj_q, 'fs', axis=0, tiled=True)]
    all_gather x3 -> x0, waiting for transfers between devices: 71.8 us -> none  [the longest x1 71.1 us: per_device(): lax.all_gather(new_weight_o.astype(jnp.bfloat16), 'fs', axis=0, tiled=True)]
    psum x1 -> x0, blocking collectives: 40.1 us -> none  [per_device(): lax.psum(jnp.sum(low_q * low_q) + jnp.sum(low_o * low_o), ('fs', 'tp'))]
    dot_general x6 -> x4, matrix products: 36.5 us -> 10.4 us  [update(): jnp.dot(basis, directions, preferred_element_type=f32) + decay_rate * weight]
    unnamed x14 -> x30, local copies, waits for them, and re-layouts: 23.1 us -> 4.98 us
  transfers between devices with their start and end apart: 5 -> 0, of which waited for: 4 -> 0; matrix products, arithmetic and copies ran while one was open for 13% -> 0% of each run, Pallas kernels for 0% -> 0%
where the time goes in v1:
time: 148 us; the launch traced here: 147 us
  Pallas kernels  124 us (84%)
  matrix products  10.4 us (7%)
  other arithmetic  6.91 us (5%)
  local copies, waits for them, and re-layouts  4.98 us (3%)
    pallas_call x1, Pallas kernels, per_device(): pl.pallas_call(functools.partial(kernel, n, tps, s, entries, tile), out_s...  124 us
    dot_general x4, matrix products, update(): jnp.dot(basis, directions, preferred_element_type=f32) + decay_rate * weight  10.4 us
    unnamed x30, local copies, waits for them, and re-layouts  4.98 us

profile of v1, /device:TPU:0, one launch (start us, length us, event | category | flops | bytes accessed | tf_op | source)
XLA Modules:
  0.0 147.3 jit_solution(5847428104163544713)
XLA Ops:
  0.6 1.8 %pad_maximum_fusion = (f32[32,1280]{1,0:T(8,128)}, f32[32,1280]{1,0:T(8,128)}) fusion(f32[32,512]{1,0:T(8,128)} %param.22, f32[32,768]{1,0:T(8,128)} %param.20, f32[32,512]{1,0:T(8,128)} %param.23, f32[32,768]{1,0:T(8,128)} %param.21), kind=kLoop, calls=%fused_computation.20 | loop fusion | flops 81920 | bytes 655360 | tf_op jit(solution)/shard_map/concatenate | solution.py:277
  2.4 2.1 %convert_element_type.25.wo_in = bf16[512,512]{1,0:T(8,128)(2,1)} convert(f32[512,512]{1,0:T(8,128)} %param.19) | non-fusion elementwise | flops 262144 | bytes 1572864 | tf_op jit(solution)/shard_map/convert_element_type | solution.py:280
  4.5 1.7 %convert_element_type.24.wq_in = bf16[128,768]{1,0:T(8,128)(2,1)} convert(f32[128,768]{1,0:T(8,128)} %param.18) | non-fusion elementwise | flops 98304 | bytes 589824 | tf_op jit(solution)/shard_map/convert_element_type | solution.py:279
  6.2 124.3 %shard_map.195 = (bf16[8,128,768]{2,1,0:T(8,128)(2,1)}, bf16[8,512,512]{2,1,0:T(8,128)(2,1)}, bf16[8,4,32,256]{3,2,1,0:T(8,128)(2,1)}, bf16[8,4,128,256]{3,2,1,0...) custom-call(bf16[1536,1024]{1,0:T(8,128)(2,1)} %ql_hbm.1, bf16[1536,768]{1,0:T(8,128)(2,1)} %gq_hbm.1, ...), custom_call_target="tpu_custom_call" | custom-call | tf_op jit(solution)/shard_map/pallas_call | solution.py:284
  130.5 0.0 copy-start.2
  130.5 0.0 copy-start.10
  130.5 6.7 %fusion.2 = bf16[4096,512]{1,0:T(8,128)(2,1)} fusion(bf16[4096,512]{1,0:T(8,128)(2,1)} %bitcast.27, bf16[4096,256]{1,0:T(8,128)(2,1)} %bitcast.28, bf16[256,1280]{1,0:T(8,128)(2,1)} %bitcast.22), kind=kOutput, calls=%fused_computation.4 | convolution fusion | flops 1086324736 | bytes 10747904 | tf_op jit(solution)/shard_map/dot_general | solution.py:346
  137.3 1.9 %fusion.5 = bf16[1024,768]{1,0:T(8,128)(2,1)} fusion(bf16[1024,768]{1,0:T(8,128)(2,1)S(1)} %bitcast.29, bf16[1024,256]{1,0:T(8,128)(2,1)S(1)} %bitcast.30, bf16[256,1280]{1,0:T(8,128)(2,1)S(1)} %bitcast.24), kind=kOutput, calls=%fused_computation.9 | convolution fusion | flops 407371776 | bytes 4063232 | tf_op jit(solution)/shard_map/dot_general | solution.py:346
  139.2 0.3 copy.25
  139.5 0.0 copy-start.1
  139.5 1.4 multiply_subtract_fusion
  141.0 0.0 copy-start.6
  141.0 1.3 copy.27
  142.3 0.0 copy-start.8
  142.3 1.3 copy.29
  143.6 0.2 copy.23
  143.8 0.0 copy-done.3
  143.8 0.0 copy-done.6
  143.8 0.3 multiply_subtract_fusion.1
  144.1 0.9 copy.26
  145.0 0.9 copy.28
  145.9 0.0 copy-done.5
  145.9 0.7 fusion.12
  146.7 0.7 fusion.13
  (16 shorter events, 0.0 us)
Async XLA Ops:
  130.5 6.8 %copy-start.2 = (bf16[8,32,1280]{2,1,0:T(8,128)(2,1)S(1)}, bf16[8,32,1280]{2,1,0:T(8,128)(2,1)}, u32[]{:S(2)}) copy-start(bf16[8,32,1280]{2,1,0:T(8,128)(2,1)} %get-tuple-element.16) | copy-start | bytes 1966084
  130.5 6.8 %copy-start.10 = (bf16[8,128,768]{2,1,0:T(8,128)(2,1)S(1)}, bf16[8,128,768]{2,1,0:T(8,128)(2,1)}, u32[]{:S(2)}) copy-start(bf16[8,128,768]{2,1,0:T(8,128)(2,1)} %get-tuple-element.18) | copy-start | bytes 4718596
  130.5 6.8 %copy-start.11 = (bf16[8,4,32,256]{3,2,1,0:T(8,128)(2,1)S(1)}, bf16[8,4,32,256]{3,2,1,0:T(8,128)(2,1)}, u32[]{:S(2)}) copy-start(bf16[8,4,32,256]{3,2,1,0:T(8,128)(2,1)} %get-tuple-element.19) | copy-start | bytes 1572868
  137.2 1.9 %copy-start = (f32[512,512]{1,0:T(8,128)S(1)}, f32[512,512]{1,0:T(8,128)}, u32[]{:S(2)}) copy-start(f32[512,512]{1,0:T(8,128)} %param.19) | copy-start | bytes 3145732
  139.5 4.1 %copy-start.1 = (f32[128,768]{1,0:T(8,128)S(1)}, f32[128,768]{1,0:T(8,128)}, u32[]{:S(2)}) copy-start(f32[128,768]{1,0:T(8,128)} %param.18) | copy-start | bytes 1179652
  141.0 2.8 %copy-start.3 = (bf16[8,32,1280]{2,1,0:T(8,128)(2,1)S(1)}, bf16[8,32,1280]{2,1,0:T(8,128)(2,1)}, u32[]{:S(2)}) copy-start(bf16[8,32,1280]{2,1,0:T(8,128)(2,1)} %get-tuple-element.16) | copy-start | bytes 1966084
  141.0 2.8 %copy-start.6 = (bf16[128,256]{1,0:T(8,128)(2,1)S(1)}, bf16[128,256]{1,0:T(8,128)(2,1)}, u32[]{:S(2)}) copy-start(bf16[128,256]{1,0:T(8,128)(2,1)} %param.16) | copy-start | bytes 196612
  142.3 3.7 %copy-start.4 = (f32[32,768]{1,0:T(8,128)S(1)}, f32[32,768]{1,0:T(8,128)}, u32[]{:S(2)}) copy-start(f32[32,768]{1,0:T(8,128)} %param.20) | copy-start | bytes 294916
  142.3 3.7 %copy-start.5 = (f32[32,768]{1,0:T(8,128)S(1)}, f32[32,768]{1,0:T(8,128)}, u32[]{:S(2)}) copy-start(f32[32,768]{1,0:T(8,128)} %param.21) | copy-start | bytes 294916
  142.3 3.7 %copy-start.9 = (f32[32,1280]{1,0:T(8,128)S(1)}, f32[32,1280]{1,0:T(8,128)}, u32[]{:S(2)}) copy-start(f32[32,1280]{1,0:T(8,128)} %get-tuple-element.17) | copy-start | bytes 491524
  142.3 4.4 %copy-start.7 = (f32[32,512]{1,0:T(8,128)S(1)}, f32[32,512]{1,0:T(8,128)}, u32[]{:S(2)}) copy-start(f32[32,512]{1,0:T(8,128)} %param.22) | copy-start | bytes 196612
  142.3 4.4 %copy-start.8 = (f32[32,512]{1,0:T(8,128)S(1)}, f32[32,512]{1,0:T(8,128)}, u32[]{:S(2)}) copy-start(f32[32,512]{1,0:T(8,128)} %param.23) | copy-start | bytes 196612

commit v2 on v1

v2 whole, which is shorter than its diff:
```python
import functools
import math

import jax
import jax.numpy as jnp
from jax import lax
from jax.experimental import pallas as pl
from jax.experimental.pallas import tpu as pltpu
from jax.sharding import PartitionSpec as P

beta_first = 0.8
beta_second = 0.9
epsilon = 1e-08
decay_rate = 2.0
step_rate = 0.05
f32 = jnp.float32
bf16 = jnp.bfloat16
MESH = pl.DeviceIdType.MESH


def moments(first, second, scaled):
    first_new = beta_first * first + (1.0 - beta_first) * scaled
    second_new = beta_second * second + (1.0 - beta_second) * scaled * scaled
    return (first_new, second_new, first_new / (jnp.sqrt(second_new) + epsilon))


def kernel(
    n,
    tps,
    s,
    entries,
    tile,
    ql_hbm,
    gq_hbm,
    ho_hbm,
    go_hbm,
    pq_in,
    po_in,
    wq_in,
    wo_in,
    first_q,
    second_q,
    first_o,
    second_o,
    wq_all,
    wo_all,
    pq_all,
    po_all,
    dir_all,
    scaled_out,
    ql,
    gq,
    ho,
    go,
    tq,
    to,
    low_send,
    low_y,
    z_send,
    z_recv,
    ss_fs,
    ss_tp,
    ss_own,
    load_sem,
    a_send,
    a_recv,
    b_send,
    b_recv,
    c_send,
    c_recv,
    w_send,
    w_recv,
    ry_send,
    ry_recv,
    rz_send,
    rz_recv,
    sf_send,
    sf_recv,
    st_send,
    st_recv,
    da_send,
    da_recv,
    db_send,
    db_recv,
):
    f = lax.axis_index("fs")
    t = lax.axis_index("tp")
    depth = min(4, n)
    width = n // depth
    z, y = f // width, lax.rem(f, width)

    def fs_at(kz, ky):
        return lax.rem(z + kz + depth, depth) * width + lax.rem(y + ky + width, width)

    mine = lax.rem(t, s)
    group = t - mine

    loads = [
        pltpu.make_async_copy(src, dst, load_sem.at[i])
        for i, (src, dst) in enumerate(((go_hbm, go), (ho_hbm, ho), (ql_hbm, ql), (gq_hbm, gq)))
    ]
    for load in loads:
        load.start()

    barrier = pltpu.get_barrier_semaphore()
    for k in range(1, n):
        pl.semaphore_signal(barrier, inc=1, device_id=(lax.rem(f + k, n), t), device_id_type=MESH)
    for k in range(1, tps):
        pl.semaphore_signal(barrier, inc=1, device_id=(f, lax.rem(t + k, tps)), device_id_type=MESH)
    wq_all[f] = wq_in[...].astype(bf16)
    wo_all[f] = wo_in[...].astype(bf16)
    pl.semaphore_wait(barrier, n + tps - 2)
    started = []

    def send(src, dst, send_sem, recv_sem, device):
        copy = pltpu.make_async_remote_copy(
            src_ref=src,
            dst_ref=dst,
            send_sem=send_sem,
            recv_sem=recv_sem,
            device_id=device,
            device_id_type=MESH,
        )
        copy.start()
        started.append(copy)
        return copy

    pairs = ((pq_in, pq_all), (po_in, po_all))
    along_z = {}
    for k in range(1, depth):
        along_z[k] = [
            send(own.at[mine], whole.at[f, mine], a_send.at[i, k], a_recv.at[i, k], (fs_at(k, 0), t))
            for i, (own, whole) in enumerate(pairs)
        ]
    along_y = {}

    def pass_y(kz):
        for ky in range(1, width):
            copies = []
            for i, (own, whole) in enumerate(pairs):
                slot = whole.at[fs_at(-kz, 0), mine]
                source = own.at[mine] if kz == 0 else slot
                copies.append(
                    send(source, slot, b_send.at[i, kz, ky], b_recv.at[i, kz, ky], (fs_at(0, ky), t))
                )
            along_y[kz, ky] = copies

    along_tp = []

    def pass_tp(kz, ky):
        for j in range(1, s):
            target = group + lax.rem(mine + j, s)
            for i, (own, whole) in enumerate(pairs):
                slot = whole.at[fs_at(-kz, -ky), mine]
                at = kz * width + ky
                along_tp.append(
                    send(slot, slot, c_send.at[i, at, j], c_recv.at[i, at, j], (f, target))
                )

    pass_y(0)

    place = y * depth + z + lax.rem(y, 2) * (depth - 1 - 2 * z)

    def at_place(p):
        p = lax.rem(p + 2 * n, n)
        py = p // depth
        r = lax.rem(p, depth)
        return (r + lax.rem(py, 2) * (depth - 1 - 2 * r)) * width + py

    parts = []
    for whole, pieces in ((wq_all, 1), (wo_all, 2)):
        half = whole.shape[1] // 2
        for piece in range(pieces):
            for way, sign in enumerate((1, -1)):
                size = half // pieces
                parts.append((whole, pl.ds(way * half + piece * size, size), sign))
    ring = []

    def ring_step(step):
        copies = []
        for i, (whole, rows, sign) in enumerate(parts):
            if step > 0:
                ring[step - 1][i].wait_recv()
            if step < n - 1:
                slot = whole.at[at_place(place - sign * step), rows]
                copies.append(
                    send(slot, slot, w_send.at[step, i], w_recv.at[step, i], (at_place(place + sign), t))
                )
        ring.append(copies)

    ring_step(0)
    for own, whole in pairs:
        whole[f] = own[...]

    for kz in range(1, depth):
        for copy in along_z[kz]:
            copy.wait_recv()
        pass_y(kz)
        pass_tp(kz, 0)
    for kz in range(depth):
        for ky in range(1, width):
            for copy in along_y[kz, ky]:
                copy.wait_recv()
            pass_tp(kz, ky)
    for load in loads:
        load.wait()
    for copy in along_tp:
        copy.wait_recv()
    ring_step(1)

    tokens = go.shape[0]
    ro = po_all.shape[2] * s
    rank = pq_all.shape[3]

    @pl.loop(0, tokens // tile)
    def _(i):
        at = pl.ds(pl.multiple_of(i * tile, tile), tile)
        acc = jnp.zeros((tile, rank), f32)
        for b in range(n):
            acc += jnp.dot(
                go[at, b * ro : (b + 1) * ro],
                po_all[b].reshape(ro, rank),
                preferred_element_type=f32,
            )
        to[:, at] = acc.T.astype(bf16)
        acc = jnp.dot(ql[at, :], pq_all[...].reshape(-1, rank), preferred_element_type=f32)
        tq[:, at] = acc.T.astype(bf16)

    cq = gq.shape[1]
    rr = low_send.shape[2]
    for left, right, base in ((tq, gq, 0), (to, ho, cq)):
        for c in range(0, right.shape[1], 128):
            part = jnp.dot(left[...], right[:, c : c + 128], preferred_element_type=f32)
            part = part.astype(bf16).reshape(depth, width, rr, 128)
            for b in range(width):
                low_send[b, :, :, base + c : base + c + 128] = part[:, b]

    sums_y = [
        send(
            low_send.at[lax.rem(y + k, width)],
            low_y.at[k],
            ry_send.at[k],
            ry_recv.at[k],
            (fs_at(0, k), t),
        )
        for k in range(1, width)
    ]
    ring_step(2)
    for copy in sums_y:
        copy.wait_recv()
    for b in range(depth):
        z_sum = low_send[y, b].astype(f32)
        for k in range(1, width):
            z_sum += low_y[k, b].astype(f32)
        z_send[b] = z_sum.astype(bf16)
    sums_z = [
        send(
            z_send.at[lax.rem(z + k, depth)],
            z_recv.at[k],
            rz_send.at[k],
            rz_recv.at[k],
            (fs_at(k, 0), t),
        )
        for k in range(1, depth)
    ]
    low = z_send[z].astype(f32)
    for copy in sums_z:
        copy.wait_recv()
    for k in range(1, depth):
        low += z_recv[k].astype(f32)
    ss_own[...] = jnp.broadcast_to(jnp.sum(low * low, keepdims=True), ss_own.shape)
    sums = [
        send(ss_own, ss_fs.at[f], sf_send.at[k], sf_recv.at[k], (lax.rem(f + k, n), t))
        for k in range(1, n)
    ]
    ss_fs[f] = ss_own[...]
    ring_step(3)
    for copy in sums:
        copy.wait_recv()
    ss_tp[t] = jnp.sum(ss_fs[...], axis=0)
    sums_tp = [
        send(ss_tp.at[t], ss_tp.at[t], st_send.at[k], st_recv.at[k], (f, lax.rem(t + k, tps)))
        for k in range(1, tps)
    ]
    for copy in sums_tp:
        copy.wait_recv()
    total = jnp.sum(ss_tp[...], axis=0)[0:1, 0:1]
    clip_scale = jnp.minimum(1.0, math.sqrt(entries) / jnp.sqrt(total))
    scaled = clip_scale * low
    scaled_out[...] = scaled
    _, _, direct = moments(first_q[...], second_q[...], scaled[:, :cq])
    dir_all[f, :, :cq] = direct.astype(bf16)
    _, _, direct = moments(first_o[...], second_o[...], scaled[:, cq:])
    dir_all[f, :, cq:] = direct.astype(bf16)

    spread = {
        k: send(dir_all.at[f], dir_all.at[f], da_send.at[k], da_recv.at[k], (fs_at(k, 0), t))
        for k in range(1, depth)
    }
    spread_y = []

    def spread_on(kz):
        slot = dir_all.at[fs_at(-kz, 0)]
        for ky in range(1, width):
            spread_y.append(
                send(slot, slot, db_send.at[kz, ky], db_recv.at[kz, ky], (fs_at(0, ky), t))
            )

    spread_on(0)
    ring_step(4)
    for k in range(1, depth):
        spread[k].wait_recv()
        spread_on(k)
    for step in range(5, n):
        ring_step(step)
    for copy in spread_y:
        copy.wait_recv()
    for copy in started:
        copy.wait_send()


def finish(
    wq_all,
    wo_all,
    pq_all,
    po_all,
    dir_all,
    scaled,
    proj_q,
    proj_o,
    weight_q,
    weight_o,
    first_q,
    second_q,
    first_o,
    second_o,
    new_weight_q,
    new_weight_o,
    first_nq,
    second_nq,
    first_no,
    second_no,
    step_q,
    step_o,
    copy_q,
    copy_o,
):
    cq = copy_q.shape[1]
    rank = proj_q.shape[1]
    direct = dir_all[...].reshape(rank, dir_all.shape[2])
    sides = ((direct[:, :cq], wq_all, pq_all, copy_q), (direct[:, cq:], wo_all, po_all, copy_o))

    def update(basis, directions, weight):
        step = jnp.dot(basis, directions, preferred_element_type=f32) + decay_rate * weight
        return step, weight - step_rate * step

    for directions, weights, bases, copy in sides:
        _, new = update(bases[0].reshape(-1, rank), directions, weights[0].astype(f32))
        copy[...] = new.astype(bf16)

    @pl.when(pl.program_id(0) == 0)
    def _():
        step_q[...], new_weight_q[...] = update(proj_q[...], direct[:, :cq], weight_q[...])
        step_o[...], new_weight_o[...] = update(proj_o[...], direct[:, cq:], weight_o[...])
        first_nq[...], second_nq[...], _ = moments(first_q[...], second_q[...], scaled[:, :cq])
        first_no[...], second_no[...], _ = moments(first_o[...], second_o[...], scaled[:, cq:])


def per_device(
    n,
    tps,
    query_latent_rows,
    grad_q,
    head_out,
    grad_out,
    proj_q,
    proj_o,
    query_up_weight,
    weight_o,
    first_q,
    second_q,
    first_o,
    second_o,
):
    rq, rank = proj_q.shape
    ro = proj_o.shape[0]
    cq, co = grad_q.shape[1], head_out.shape[1]
    rr = first_q.shape[0]
    tokens = grad_out.shape[0]
    columns = cq + co
    s = math.gcd(tps, rq // 16)
    depth = min(4, n)
    width = n // depth
    tile = math.gcd(tokens, 256)
    entries = rr * n * columns * tps
    vmem = pl.BlockSpec(memory_space=pltpu.VMEM)
    hbm = pl.BlockSpec(memory_space=pl.ANY)
    dma = pltpu.SemaphoreType.DMA

    def both(*shape):
        return [dma(shape), dma(shape)]

    own = (first_q, second_q, first_o, second_o)
    gathered = pl.pallas_call(
        functools.partial(kernel, n, tps, s, entries, tile),
        out_shape=(
            jax.ShapeDtypeStruct((n, rq, cq), bf16),
            jax.ShapeDtypeStruct((n, ro, co), bf16),
            jax.ShapeDtypeStruct((n, s, rq // s, rank), bf16),
            jax.ShapeDtypeStruct((n, s, ro // s, rank), bf16),
            jax.ShapeDtypeStruct((n, rr, columns), bf16),
            jax.ShapeDtypeStruct((rr, columns), f32),
        ),
        in_specs=[hbm] * 4 + [vmem] * 8,
        out_specs=(vmem,) * 6,
        scratch_shapes=[
            pltpu.VMEM(query_latent_rows.shape, bf16),
            pltpu.VMEM(grad_q.shape, bf16),
            pltpu.VMEM(head_out.shape, bf16),
            pltpu.VMEM(grad_out.shape, bf16),
            pltpu.VMEM((rank, tokens), bf16),
            pltpu.VMEM((rank, tokens), bf16),
            pltpu.VMEM((width, depth, rr, columns), bf16),
            pltpu.VMEM((width, depth, rr, columns), bf16),
            pltpu.VMEM((depth, rr, columns), bf16),
            pltpu.VMEM((depth, rr, columns), bf16),
            pltpu.VMEM((n, 8, 128), f32),
            pltpu.VMEM((tps, 8, 128), f32),
            pltpu.VMEM((8, 128), f32),
            dma((4,)),
            *both(2, depth),
            *both(2, depth, width),
            *both(2, n, s),
            *both(n - 1, 6),
            *both(width),
            *both(depth),
            *both(n),
            *both(tps),
            *both(depth),
            *both(depth, width),
        ],
        compiler_params=pltpu.CompilerParams(
            collective_id=0, has_side_effects=True, vmem_limit_bytes=60 * 1024 * 1024
        ),
    )(
        query_latent_rows,
        grad_q,
        head_out,
        grad_out,
        proj_q.reshape(s, rq // s, rank),
        proj_o.reshape(s, ro // s, rank),
        query_up_weight,
        weight_o,
        *own,
    )

    def whole(shape):
        return pl.BlockSpec(shape, lambda i: (0,) * len(shape))

    def rows_of(shape):
        return pl.BlockSpec((1, *shape[1:]), lambda i: (i,) + (0,) * (len(shape) - 1))

    held = (proj_q, proj_o, query_up_weight, weight_o, *own)
    outs = (query_up_weight, weight_o, first_q, second_q, first_o, second_o, query_up_weight, weight_o)
    return pl.pallas_call(
        finish,
        grid=(n,),
        out_shape=tuple(jax.ShapeDtypeStruct(a.shape, f32) for a in outs)
        + (jax.ShapeDtypeStruct((n * rq, cq), bf16), jax.ShapeDtypeStruct((n * ro, co), bf16)),
        in_specs=[rows_of(a.shape) for a in gathered[:4]]
        + [whole(a.shape) for a in (*gathered[4:], *held)],
        out_specs=tuple(whole(a.shape) for a in outs)
        + (pl.BlockSpec((rq, cq), lambda i: (i, 0)), pl.BlockSpec((ro, co), lambda i: (i, 0))),
        compiler_params=pltpu.CompilerParams(vmem_limit_bytes=48 * 1024 * 1024),
    )(*gathered, *held)


def solution(mesh):
    both = P("fs", "tp")
    rows = P("fs", None)
    return jax.shard_map(
        functools.partial(per_device, mesh.shape["fs"], mesh.shape["tp"]),
        mesh=mesh,
        in_specs=(rows, both, both, rows, rows, rows) + (both,) * 6,
        out_specs=(both,) * 8 + (P(None, "tp"),) * 2,
        check_vma=False,
    )
```

time: 148 us -> 125 us (0.84)
  matrix products: 10.4 us -> 0 us
  other arithmetic: 6.91 us -> 0 us
  Pallas kernels: 124 us -> 119 us
    pallas_call x1, Pallas kernels: 124 us -> 109 us  [per_device(): pl.pallas_call(functools.partial(kernel, n, tps, s, entries, tile), out_s...]
    dot_general x4 -> x0, matrix products: 10.4 us -> none  [update(): jnp.dot(basis, directions, preferred_element_type=f32) + decay_rate * weight]
    pallas_call x0 -> x1, Pallas kernels: none -> 10.2 us  [per_device(): pl.pallas_call(finish, grid=(n,), out_shape=tuple((jax.ShapeDtypeStruct(a...]
    convert_element_type x2 -> x0, other arithmetic: 3.77 us -> none  [the longest x1 2.08 us: per_device(): wo = weight_o.astype(bf16)]
    concatenate x1 -> x0, other arithmetic: 1.76 us -> none  [per_device(): first = jnp.concatenate([first_q, first_o], axis=1)]
    unnamed x30 -> x24, local copies, waits for them, and re-layouts: 4.98 us -> 4.48 us
where the time goes in v2:
time: 125 us; the launch traced here: 124 us
  Pallas kernels  119 us (95%)
  local copies, waits for them, and re-layouts  4.48 us (4%)
    pallas_call x1, Pallas kernels, per_device(): pl.pallas_call(functools.partial(kernel, n, tps, s, entries, tile), out_s...  109 us
    pallas_call x1, Pallas kernels, per_device(): pl.pallas_call(finish, grid=(n,), out_shape=tuple((jax.ShapeDtypeStruct(a...  10.2 us
    unnamed x24, local copies, waits for them, and re-layouts  4.48 us

profile of v2, /device:TPU:0, one launch (start us, length us, event | category | flops | bytes accessed | tf_op | source)
XLA Modules:
  0.0 124.4 jit_solution(9833193562514770828)
XLA Ops:
  0.6 0.0 copy-start
  0.7 0.0 copy-start.1
  0.7 0.0 copy-start.3
  0.7 0.0 copy-start.6
  0.7 0.0 copy-start.7
  0.7 0.0 copy-start.8
  0.7 0.0 copy-start.9
  0.7 0.0 copy-start.10
  0.7 109.0 %shard_map.195 = (bf16[8,128,768]{2,1,0:T(8,128)(2,1)}, bf16[8,512,512]{2,1,0:T(8,128)(2,1)}, bf16[8,4,32,256]{3,2,1,0:T(8,128)(2,1)}, bf16[8,4,128,256]{3,2,1,0...) custom-call(bf16[1536,1024]{1,0:T(8,128)(2,1)} %ql_hbm.1, bf16[1536,768]{1,0:T(8,128)(2,1)} %gq_hbm.1, ...), custom_call_target="tpu_custom_call" | custom-call | tf_op jit(solution)/shard_map/pallas_call | solution.py:404
  109.7 0.0 copy-done
  109.7 0.0 copy-done.1
  109.7 0.0 copy-done.3
  109.7 0.0 copy-done.6
  109.7 0.0 copy-done.7
  109.8 0.0 copy-done.8
  109.8 0.0 copy-done.9
  109.8 0.0 copy-done.10
  109.8 0.0 copy-start.2
  109.8 1.4 %copy-done.2 = bf16[8,128,768]{2,1,0:T(8,128)(2,1)S(1)} copy-done((bf16[8,128,768]{2,1,0:T(8,128)(2,1)S(1)}, bf16[8,128,768]{2,1,0:T(8,128)(2,1)}, u32[]{:S(2)}) %copy-start.2) | copy-done | bytes 1572888
  111.2 0.0 copy-start.4
  111.2 1.1 copy-done.4
  112.3 1.0 copy-done.5
  113.3 0.9 copy-done.11
  114.2 10.2 %shard_map.196 = (f32[128,768]{1,0:T(8,128)}, f32[512,512]{1,0:T(8,128)}, f32[32,768]{1,0:T(8,128)}, f32[32,768]{1,0:T(8,128)}, f32[32,512]{1,0:T(8,128)}, /*ind...) custom-call(bf16[8,128,768]{2,1,0:T(8,128)(2,1)S(1)} %copy-done.2, ...), custom_call_target="tpu_custom_call" | custom-call | tf_op jit(solution)/shard_map/pallas_call | solution.py:465
  (2 shorter events, 0.0 us)
Async XLA Ops:
  0.6 109.1 %copy-start = (f32[512,512]{1,0:T(8,128)S(1)}, f32[512,512]{1,0:T(8,128)}, u32[]{:S(2)}) copy-start(f32[512,512]{1,0:T(8,128)} %weight_o.1) | copy-start | bytes 3145732
  0.7 109.1 %copy-start.1 = (f32[128,768]{1,0:T(8,128)S(1)}, f32[128,768]{1,0:T(8,128)}, u32[]{:S(2)}) copy-start(f32[128,768]{1,0:T(8,128)} %weight_q.1) | copy-start | bytes 1179652
  0.7 109.1 %copy-start.3 = (bf16[512,256]{1,0:T(8,128)(2,1)S(1)}, bf16[512,256]{1,0:T(8,128)(2,1)}, u32[]{:S(2)}) copy-start(bf16[512,256]{1,0:T(8,128)(2,1)} %proj_o.1) | copy-start | bytes 786436
  0.7 109.1 %copy-start.6 = (f32[32,768]{1,0:T(8,128)S(1)}, f32[32,768]{1,0:T(8,128)}, u32[]{:S(2)}) copy-start(f32[32,768]{1,0:T(8,128)} %first_q.3) | copy-start | bytes 294916
  0.7 109.1 %copy-start.7 = (f32[32,768]{1,0:T(8,128)S(1)}, f32[32,768]{1,0:T(8,128)}, u32[]{:S(2)}) copy-start(f32[32,768]{1,0:T(8,128)} %second_q.3) | copy-start | bytes 294916
  0.7 109.1 %copy-start.8 = (bf16[128,256]{1,0:T(8,128)(2,1)S(1)}, bf16[128,256]{1,0:T(8,128)(2,1)}, u32[]{:S(2)}) copy-start(bf16[128,256]{1,0:T(8,128)(2,1)} %proj_q.1) | copy-start | bytes 196612
  0.7 109.1 %copy-start.9 = (f32[32,512]{1,0:T(8,128)S(1)}, f32[32,512]{1,0:T(8,128)}, u32[]{:S(2)}) copy-start(f32[32,512]{1,0:T(8,128)} %first_o.3) | copy-start | bytes 196612
  0.7 109.1 %copy-start.10 = (f32[32,512]{1,0:T(8,128)S(1)}, f32[32,512]{1,0:T(8,128)}, u32[]{:S(2)}) copy-start(f32[32,512]{1,0:T(8,128)} %second_o.3) | copy-start | bytes 196612
  109.8 1.4 %copy-start.2 = (bf16[8,128,768]{2,1,0:T(8,128)(2,1)S(1)}, bf16[8,128,768]{2,1,0:T(8,128)(2,1)}, u32[]{:S(2)}) copy-start(bf16[8,128,768]{2,1,0:T(8,128)(2,1)} %get-tuple-element.16.wq_all) | copy-start | bytes 4718596
  111.2 1.1 copy-start.4
  112.3 1.0 copy-start.5
  113.3 0.9 copy-start.11
